TPU v7x, 32 devices: a whole 2x2x4 slice. The times are simulated.
32 devices in a mesh: ep: 4 (over y, x), tp: 8 (over z, core).
Axes of the slice: x: 2, y: 2, z: 4, core: 2. Of those that a mesh axis runs over, the one named last changes fastest.
Arguments:
- tokens: bfloat16 [64, 4096], P(None, 'ep'), may hold values from -60 to 60
- gain_attn: bfloat16 [4096], P('ep'), may hold values from 0.099609375 to 1.8984375
- w_query: bfloat16 [4096, 2048], P('ep', 'tp'), may hold values from -0.09375 to 0.09375
- w_key: bfloat16 [4096, 2048], P('ep', 'tp'), may hold values from -0.09375 to 0.09375
- w_value: bfloat16 [4096, 2048], P('ep', 'tp'), may hold values from -0.09375 to 0.09375
- w_output: bfloat16 [2048, 4096], P('tp', 'ep'), may hold values from -0.125 to 0.125
- key_cache: bfloat16 [64, 1024, 2048], P('ep', None, 'tp'), may hold values from -6 to 6
- value_cache: bfloat16 [64, 1024, 2048], P('ep', None, 'tp'), may hold values from -10 to 10
- lengths: int32 [64], P('ep'), may hold values from 128 to 1024
- score_shift: float32 [16], P('tp'), may hold values from -9.5 to -3.5
- gain_ffn: bfloat16 [4096], replicated, may hold values from 0.099609375 to 1.8984375
- w_mix: bfloat16 [4096], P('ep'), may hold values from -0.09375 to 0.09375
- w_dense_gate: bfloat16 [4096, 4096], P('ep', 'tp'), may hold values from -0.09375 to 0.09375
- w_dense_up: bfloat16 [4096, 4096], P('ep', 'tp'), may hold values from -0.09375 to 0.09375
- w_dense_down: bfloat16 [4096, 4096], P('tp', 'ep'), may hold values from -0.09375 to 0.09375
- route_group: int32 [64], replicated, may hold values from 0 to 3, as said below
- route_inner: int32 [64, 2], replicated, may hold values from 0 to 3, as said below
- route_weight: float32 [64, 2], replicated, may hold values from 0.3 to 1
- w_exp_gate: bfloat16 [16, 4096, 2048], P('ep', None, 'tp'), may hold values from -0.09375 to 0.09375
- w_exp_up: bfloat16 [16, 4096, 2048], P('ep', None, 'tp'), may hold values from -0.09375 to 0.09375
- w_exp_down: bfloat16 [16, 2048, 4096], P('ep', 'tp'), may hold values from -0.125 to 0.125
Outputs:
- mixed: bfloat16 [64, 4096], P(None, 'ep')
- new_keys: bfloat16 [64, 2048], P('ep', 'tp')
- new_values: bfloat16 [64, 2048], P('ep', 'tp')
Inputs may be any that keep to these rules, and one draw needn't show every extreme that they name: `route_group`: within every aligned block of 16 sequences (the sequences of one index of ep) exactly half of the tokens use one group, the same group in every block; the other groups share the rest. A token's 2 experts inside its group differ. Within every aligned block of 16 sequences no expert (route_group * 4 + route_inner) is used by more than 4 tokens, and the experts of the group that half of the block uses are each used by exactly 4.
All inputs are finite; a program needn't handle non-finite values.
Results may differ from a plain program's by a relative error of at most 0.0039.
The roundings to bfloat16 on the way count: a program that leaves them out, or rounds other values in their place, can miss the bound.
Values may be sent and summed in bfloat16 or wider, within the bound.
A program may use at most 128 MiB of HBM per device.

v0:
```python
import math
import jax
import jax.numpy as jnp
from jax import lax
from jax.sharding import PartitionSpec as P

D = 4096
HD = 128
EPG = 4
TOPK = 2
EXPERTS = 16
CAP = 4
norm_eps = 1e-06


def on_device(
    tokens,
    gain_attn,
    w_query,
    w_key,
    w_value,
    w_output,
    key_cache,
    value_cache,
    lengths,
    score_shift,
    gain_ffn,
    w_mix,
    w_dense_gate,
    w_dense_up,
    w_dense_down,
    route_group,
    route_inner,
    route_weight,
    w_exp_gate,
    w_exp_up,
    w_exp_down,
):
    ep_count = lax.axis_size("ep")
    batch_all, col_width = tokens.shape
    seq_local = batch_all // ep_count
    head_cols = w_query.shape[1]
    heads_local = head_cols // HD
    tokens_float = tokens.astype(jnp.float32)
    squares = lax.psum_scatter(
        jnp.sum(tokens_float * tokens_float, axis=1), "ep", scatter_dimension=0, tiled=True
    )
    inv_first = lax.rsqrt(squares / D + norm_eps)[:, None]
    scaled_in = (tokens_float * gain_attn.astype(jnp.float32)).astype(jnp.bfloat16)
    w_joint = jnp.concatenate([w_query, w_key, w_value], axis=1)
    joint_proj = (
        lax.psum_scatter(
            jnp.dot(scaled_in, w_joint, preferred_element_type=jnp.float32),
            "ep",
            scatter_dimension=0,
            tiled=True,
        )
        * inv_first
    )
    queries = joint_proj[:, :head_cols].astype(jnp.bfloat16)
    new_keys = joint_proj[:, head_cols : 2 * head_cols].astype(jnp.bfloat16)
    new_values = joint_proj[:, 2 * head_cols :].astype(jnp.bfloat16)
    cache_len = key_cache.shape[1]
    head_query = queries.reshape(seq_local, heads_local, HD)
    head_keys = key_cache.reshape(seq_local, cache_len, heads_local, HD)
    scores = jnp.einsum(
        "bhd,blhd->bhl", head_query, head_keys, preferred_element_type=jnp.float32
    ) / math.sqrt(HD)
    scores = scores + score_shift[None, :, None]
    live_mask = lax.broadcasted_iota(jnp.int32, scores.shape, 2) < lengths[:, None, None]
    soft_terms = jnp.where(live_mask, jax.nn.softplus(scores), 0.0)
    later_sum = lax.cumsum(soft_terms, axis=2, reverse=True) - soft_terms
    stick = jnp.where(live_mask, jnp.exp(jax.nn.log_sigmoid(scores) - later_sum), 0.0).astype(
        jnp.bfloat16
    )
    head_values = value_cache.reshape(seq_local, cache_len, heads_local, HD)
    attended = jnp.einsum("bhl,blhd->bhd", stick, head_values, preferred_element_type=jnp.float32)
    attended = attended.reshape(seq_local, head_cols).astype(jnp.bfloat16)
    attn_part = jnp.dot(
        lax.all_gather(attended, "ep", axis=0, tiled=True),
        w_output,
        preferred_element_type=jnp.float32,
    )
    attn_out = lax.psum(attn_part, "tp")
    middle = (tokens_float + attn_out).astype(jnp.bfloat16)
    middle_float = middle.astype(jnp.float32)
    gain_float = gain_ffn.astype(jnp.float32)
    gain_cols = lax.dynamic_slice_in_dim(gain_float, lax.axis_index("ep") * col_width, col_width, 0)
    scaled_mid = (middle_float * gain_cols).astype(jnp.bfloat16)
    dense_pre, dense_lin, mix_pre, mid_squares = lax.psum(
        (
            jnp.dot(scaled_mid, w_dense_gate, preferred_element_type=jnp.float32),
            jnp.dot(scaled_mid, w_dense_up, preferred_element_type=jnp.float32),
            jnp.dot(scaled_mid, w_mix, preferred_element_type=jnp.float32),
            jnp.sum(middle_float * middle_float, axis=1),
        ),
        "ep",
    )
    inv_second = lax.rsqrt(mid_squares / D + norm_eps)[:, None]
    dense_hidden = (jax.nn.silu(dense_pre * inv_second) * (dense_lin * inv_second)).astype(
        jnp.bfloat16
    )
    mix_gate = jax.nn.sigmoid(mix_pre * inv_second[:, 0])
    dense_part = (
        jnp.dot(dense_hidden, w_dense_down, preferred_element_type=jnp.float32) * mix_gate[:, None]
    )
    slot_count = CAP * ep_count
    expert_ids = (route_group[:, None] * EPG + route_inner).reshape(-1)
    expert_onehot = (expert_ids[:, None] == jnp.arange(EXPERTS, dtype=jnp.int32)[None, :]).astype(
        jnp.int32
    )
    per_block = expert_onehot.reshape(ep_count, seq_local * TOPK, EXPERTS)
    earlier = (jnp.cumsum(per_block, axis=1) - per_block).reshape(-1, EXPERTS)
    slot_rank = jnp.sum(earlier * expert_onehot, axis=1)
    route_index = jnp.arange(batch_all * TOPK, dtype=jnp.int32)
    block_of = route_index // (seq_local * TOPK)
    slot_flat = expert_ids * slot_count + block_of * CAP + slot_rank
    slot_table = (
        jnp.full((EXPERTS * slot_count,), batch_all, jnp.int32)
        .at[slot_flat]
        .set(route_index // TOPK)
    )
    padded_middle = jnp.concatenate([middle, jnp.zeros((1, col_width), jnp.bfloat16)], axis=0)
    outgoing = jnp.take(padded_middle, slot_table, axis=0).reshape(EXPERTS, slot_count, col_width)
    arrived_float = lax.all_to_all(outgoing, "ep", split_axis=0, concat_axis=2, tiled=True).astype(
        jnp.float32
    )
    inv_rows = lax.rsqrt(jnp.mean(arrived_float * arrived_float, axis=2, keepdims=True) + norm_eps)
    scaled_rows = (arrived_float * gain_float).astype(jnp.bfloat16)
    gate_pre = (
        jnp.einsum("end,edf->enf", scaled_rows, w_exp_gate, preferred_element_type=jnp.float32)
        * inv_rows
    )
    up_proj = (
        jnp.einsum("end,edf->enf", scaled_rows, w_exp_up, preferred_element_type=jnp.float32)
        * inv_rows
    )
    hidden = (jax.nn.silu(gate_pre) * up_proj).astype(jnp.bfloat16)
    expert_rows = jnp.einsum("enf,efd->end", hidden, w_exp_down, preferred_element_type=jnp.float32)
    returned = lax.all_to_all(expert_rows, "ep", split_axis=2, concat_axis=0, tiled=True)
    flat_back = returned.reshape(EXPERTS * slot_count, col_width)
    routed = jnp.take(flat_back, slot_flat, axis=0).reshape(batch_all, TOPK, col_width)
    expert_part = jnp.sum(routed * route_weight[:, :, None], axis=1)
    result_sum = middle_float + lax.psum(expert_part + dense_part, "tp")
    return (result_sum.astype(jnp.bfloat16), new_keys, new_values)


def solution(mesh):
    placed = (
        P(None, "ep"),
        P("ep"),
        P("ep", "tp"),
        P("ep", "tp"),
        P("ep", "tp"),
        P("tp", "ep"),
        P("ep", None, "tp"),
        P("ep", None, "tp"),
        P("ep"),
        P("tp"),
        P(),
        P("ep"),
        P("ep", "tp"),
        P("ep", "tp"),
        P("tp", "ep"),
        P(),
        P(),
        P(),
        P("ep", None, "tp"),
        P("ep", None, "tp"),
        P("ep", "tp", None),
    )
    return jax.shard_map(
        on_device,
        mesh=mesh,
        in_specs=placed,
        out_specs=(P(None, "ep"), P("ep", "tp"), P("ep", "tp")),
        check_vma=False,
    )
```

profile of v0, /device:TPU:0, one launch (start us, length us, event | category | flops | bytes accessed | tf_op | source)
XLA Modules:
  0.0 316.2 jit_solution(12506751394663622789)
XLA Ops:
  7.2 0.8 convert_element_type.69
  8.0 2.5 fusion.3
  10.6 1.0 fusion.14
  11.7 12.3 %copy.64 = bf16[16,1024,256]{1,2,0:T(8,128)(2,1)} copy(bf16[16,1024,256]{2,1,0:T(8,128)(2,1)} %param.27) | data formatting | bytes 16777216 | tf_op jit(solution)/shard_map/reshape | solution.py:65
  24.0 0.1 copy.50
  24.1 0.1 eq.19
  24.2 0.1 fusion.41
  24.3 0.1 reduce_window_sum.27
  24.4 0.2 select_reduce_fusion
  24.6 0.1 reduce_sum.59
  24.7 0.1 copy.53
  24.8 0.1 mul.169
  24.9 0.6 dynamic-slice
  26.2 1.0 scatter_custom_fusion
  27.2 11.5 %all-reduce.1 = f32[64]{0:T(128)S(1)} all-reduce(f32[64]{0:T(128)S(1)} %fusion.14), channel_id=3, replica_groups=mesh['ep'=4,'tp'=8] {'ep'}, use_global_device_ids=true, to_apply=%region_2.0.clone | all-reduce | flops 64 | bytes 512
  38.7 0.1 fusion.52
  38.8 0.9 multiply_convert_fusion.6
  39.7 0.6 fusion.57
  40.3 4.6 %fusion.58 = f32[16,2,1,1024]{3,2,1,0:T(1,128)S(1)} fusion(bf16[16,2,128,1]{2,3,1,0:T(2,128)(2,1)S(1)} %reshape.226, bf16[16,1024,2,128]{1,3,2,0:T(8,128)(2,1)} %bitcast.59), kind=kOutput, calls=%fused_computation.104 | convolution fusion | flops 8388608 | bytes 8527872 | tf_op jit(solution)/shard_map/bhd,blhd->bhl/dot_general | solution.py:66
  44.9 0.4 fusion.24
  45.3 0.1 reshape.188
  45.4 39.6 %reduce-window.6 = f32[16,2,8,128]{3,2,1,0:T(8,128)S(1)} reduce-window(f32[16,2,8,128]{3,2,1,0:T(8,128)S(1)} %reshape.188, f32[]{:T(128)} %constant.94.clone.1), window={size=1x1x1x128 pad=0_0x0_0x0_0x0_127}, to_apply=%region_3.4 | reduce-window | flops 4161536 | bytes 262148 | tf_op jit(solution)/shard_map/reduce-window
  85.0 0.2 copy.48
  85.3 0.1 copy.49
  85.3 0.1 broadcast_add_fusion
  85.4 0.1 reduce_window_sum.26
  85.5 0.8 fusion.42
  86.4 4.6 %fusion = f32[16,2,1,128]{3,2,1,0:T(1,128)S(1)} fusion(bf16[16,2,1024,1]{2,1,0,3:T(2,128)(2,1)S(1)} %fusion.42, bf16[16,1024,256]{2,1,0:T(8,128)(2,1)} %param.28), kind=kOutput, calls=%fused_computation.3 | convolution fusion | flops 8388608 | bytes 8470528 | tf_op jit(solution)/shard_map/bhl,blhd->bhd/dot_general | solution.py:77
  91.0 7.1 %all_gather.3 = bf16[64,256]{1,0:T(8,128)(2,1)S(1)} all-gather(bf16[16,256]{1,0:T(8,128)(2,1)S(1)} %bitcast.70), channel_id=1, replica_groups=mesh['ep'=4,'tp'=8] {'ep'}, dimensions={0}, use_global_device_ids=true | all-gather | bytes 40960 | tf_op jit(solution)/shard_map/all_gather | solution.py:80
  98.1 0.9 fusion.59
  99.1 0.1 broadcast_in_dim.46
  99.2 55.8 %all-reduce.8.cloned.1.call-done = f32[64,1024]{1,0:T(8,128)} async-done(((f32[64,1024]{1,0:T(8,128)}), f32[64,1024]{1,0:T(8,128)}) %all-reduce.8.cloned.1.call-update) | async-done | bytes 262160 | tf_op jit(solution)/shard_map/psum | solution.py:84
  154.9 1.1 fusion.17
  156.0 1.2 gather_fusion
  157.2 0.9 broadcast_select_fusion
  158.1 3.6 %all-to-all-start = ((bf16[16,16,1024]{2,1,0:T(8,128)(2,1)}), bf16[16,16,1024]{2,1,0:T(8,128)(2,1)S(1)}, u32[]{:S(2)}, u32[]{:S(2)}) async-start(bf16[16,16,1024]{2,1,0:T(8,128)(2,1)} %broadcast_select_fusion), calls=%async_computation.1 | async-start | bytes 1048576 | tf_op jit(solution)/shard_map/all_to_all | solution.py:125
  161.8 0.1 reduce_sum.58
  161.9 0.1 copy.51
  162.0 0.1 copy.52
  162.1 0.1 copy.57
  162.3 6.1 %all-to-all-done = bf16[16,16,1024]{2,1,0:T(8,128)(2,1)S(1)} async-done(((bf16[16,16,1024]{2,1,0:T(8,128)(2,1)}), bf16[16,16,1024]{2,1,0:T(8,128)(2,1)S(1)}, u32[]{:S(2)}, u32[]{:S(2)}) %all-to-all-start) | async-done | bytes 524320 | tf_op jit(solution)/shard_map/all_to_all | solution.py:125
  168.4 1.5 copy.82
  169.8 1.9 reshape.192
  171.8 0.2 multiply_reduce_fusion
  172.0 4.5 %convolution_multiply_fusion.2 = f32[4,16,256]{2,1,0:T(8,128)S(1)} fusion(bf16[4,4096,256]{2,1,0:T(8,128)(2,1)} %param.39, f32[4,16,4096]{2,1,0:T(8,128)S(1)} %reshape.192, f32[4096]{0:T(1024)S(1)} %convert_element_type.81, f32[4,16]{1,0:T(4,128)S(1)} %add_rsqrt_fusion), kind=kOutput, calls=%fused_computation.16 | convolution fusion | flops 134758400 | bytes 9519360 | tf_op jit(solution)/shard_map/end,edf->enf/dot_general | solution.py:131
  176.5 8.1 %fusion.12 = f32[4,16,4096]{2,1,0:T(8,128)S(1)} fusion(bf16[4,256,4096]{2,1,0:T(8,128)(2,1)} %param.41, bf16[4,4096,256]{2,1,0:T(8,128)(2,1)} %param.40, f32[4,16,4096]{2,1,0:T(8,128)S(1)} %reshape.192, f32[4096]{0:T(1024)S(1)} %convert_element_type.81, f32[4,16,256]{2,1,0:T(8,128)S(1)} %convolution_multiply_fusion.2, f32[4,16]{1,0:T(4,128)S(1)} %add_rsqrt_fusion), kind=kOutput, calls=%fused_computation.22 | convolution fusion | flops 269074432 | bytes 18956544 | tf_op jit(solution)/shard_map/enf,efd->end/dot_general | solution.py:139
  184.6 5.9 %copy.55 = f32[4,16,4096]{1,0,2:T(4,128)} copy(f32[4,16,4096]{2,1,0:T(8,128)S(1)} %fusion.12) | data formatting | bytes 2097152 | tf_op jit(solution)/shard_map/enf,efd->end/dot_general | solution.py:139
  190.5 8.8 %reshape.230 = f32[4,1,65536]{2,1,0:T(1,128)} reshape(f32[4096,4,16]{2,1,0:T(4,128)} %bitcast.60) | data formatting | bytes 2097152
  199.3 3.5 %all-to-all-start.1 = ((f32[4,1,65536]{2,1,0:T(1,128)}), f32[4,1,65536]{2,1,0:T(1,128)S(1)}, u32[]{:S(2)}, u32[]{:S(2)}) async-start(f32[4,1,65536]{2,1,0:T(1,128)} %reshape.230), calls=%async_computation.2 | async-start | bytes 2097152 | tf_op jit(solution)/shard_map/all_to_all | solution.py:140
  202.9 0.9 fusion.30
  203.8 2.2 fusion.32
  206.1 0.1 convolution_bitcast_fusion
  206.2 10.6 %all-reduce.2 = (f32[64]{0:T(128)S(1)}, f32[64]{0:T(128)S(1)}) all-reduce(f32[64]{0:T(128)S(1)} %convolution_bitcast_fusion, f32[64]{0:T(128)S(1)} %get-tuple-element.7), channel_id=1, replica_groups=mesh['ep'=4,'tp'=8] {'ep'}, use_global_device_ids=true, to_apply=%region_16.17 | all-reduce | flops 128 | bytes 1024 | tf_op jit(solution)/shard_map/psum | solution.py:90
  216.9 0.6 broadcast.214
  217.5 3.7 %reduce.5 = f32[4,65536]{1,0:T(4,128)S(1)} reduce(f32[4,1,65536]{2,1,0:T(1,128)S(1)} %all-to-all-done.1, f32[]{:T(128)} %broadcast.214), dimensions={1}, to_apply=%all_to_all.9.reduce_sub_computation | reduce | bytes 2097156 | tf_op jit(solution)/shard_map/all_to_all | solution.py:140
  221.2 9.1 %reshape.231 = f32[4096,4,16]{2,1,0:T(4,128)} reshape(f32[4,65536]{1,0:T(4,128)S(1)} %reduce.5) | data formatting | bytes 2097152
  230.3 6.7 %copy.56 = f32[4,16,4,1024]{3,1,0,2:T(8,128)S(1)} copy(f32[4,16,4,1024]{1,0,3,2:T(4,128)} %bitcast.61) | data formatting | bytes 2097152 | tf_op jit(solution)/shard_map/all_to_all | solution.py:140
  236.9 0.8 gather_fusion.1
  237.7 0.3 gather.15
  238.1 0.8 multiply_reduce_fusion.1
  238.9 11.5 %all-reduce.12.cloned.1.call-done = (f32[64,512]{1,0:T(8,128)}, f32[64,512]{1,0:T(8,128)}) async-done(((f32[64,512]{1,0:T(8,128)}, f32[64,512]{1,0:T(8,128)}), (f32[64,512]{1,0:T(8,128)}, f32[64,512]{1,0:T(8,128)})) %all-reduce.12.cloned.1.call-update) | async-done | bytes 262160 | tf_op jit(solution)/shard_map/psum | solution.py:90
  250.4 2.0 fusion.9
  252.5 55.6 %all-reduce.10.cloned.1.call-done = f32[64,1024]{1,0:T(8,128)} async-done(((f32[64,1024]{1,0:T(8,128)}), f32[64,1024]{1,0:T(8,128)}) %all-reduce.10.cloned.1.call-update) | async-done | bytes 262160 | tf_op jit(solution)/shard_map/psum | solution.py:144
  308.1 1.6 fusion.18
  (55 shorter events, 0.5 us)
Async XLA Ops:
  7.2 243.3 %copy-start = (bf16[512,1024]{1,0:T(8,128)(2,1)S(1)}, bf16[512,1024]{1,0:T(8,128)(2,1)}, u32[]{:S(2)}) copy-start(bf16[512,1024]{1,0:T(8,128)(2,1)} %param.35) | copy-start | bytes 3145732
  7.2 31.6 %reduce-scatter.2.cloned.1.call-start = ((), (), s32[]{:S(2)}) async-start(), calls=%async_computation.3 | async-start | bytes 245760 | tf_op jit(solution)/shard_map/reduce_scatter | solution.py:52
  10.5 144.4 %all-reduce.8.cloned.1.call-start = ((), (), s32[]{:S(2)}) async-start(), calls=%async_computation.4 | async-start | bytes 524288 | tf_op jit(solution)/shard_map/psum | solution.py:84
  11.6 12.3 %copy-start.10 = (s32[64]{0:T(128)S(1)}, s32[64]{0:T(128)}, u32[]{:S(2)}) copy-start(s32[64]{0:T(128)} %param.36) | copy-start | bytes 772
  11.6 12.3 %copy-start.8 = (s32[64,2]{0,1:T(2,128)S(1)}, s32[64,2]{0,1:T(2,128)}, u32[]{:S(2)}) copy-start(s32[64,2]{0,1:T(2,128)} %param.37) | copy-start | bytes 1540
  11.6 13.3 %copy-start.11 = (u32[32]{0:T(128)S(1)}, u32[32]{0:T(128)}, u32[]{:S(2)}) copy-start(u32[32]{0:T(128)} %constant.122) | copy-start | bytes 388
  24.0 20.9 %copy-start.5 = (s32[16]{0:T(128)S(1)}, s32[16]{0:T(128)}, u32[]{:S(2)}) copy-start(s32[16]{0:T(128)} %param.29) | copy-start | bytes 196
  24.0 20.9 %copy-start.6 = (f32[2]{0:T(128)S(1)}, f32[2]{0:T(128)}, u32[]{:S(2)}) copy-start(f32[2]{0:T(128)} %param.30) | copy-start | bytes 28
  44.9 53.3 %copy-start.3 = (bf16[256,1024]{1,0:T(8,128)(2,1)S(1)}, bf16[256,1024]{1,0:T(8,128)(2,1)}, u32[]{:S(2)}) copy-start(bf16[256,1024]{1,0:T(8,128)(2,1)} %param.26) | copy-start | bytes 1572868
  44.9 110.1 %copy-start.2 = (bf16[64,1024]{1,0:T(8,128)(2,1)S(1)}, bf16[64,1024]{1,0:T(8,128)(2,1)}, u32[]{:S(2)}) copy-start(bf16[64,1024]{1,0:T(8,128)(2,1)} %param.21) | copy-start | bytes 393220
  86.3 75.5 %copy-start.4 = (bf16[4096]{0:T(1024)(128)(2,1)S(1)}, bf16[4096]{0:T(1024)(128)(2,1)}, u32[]{:S(2)}) copy-start(bf16[4096]{0:T(1024)(128)(2,1)} %param.31) | copy-start | bytes 24580
  86.4 75.8 %copy-start.9 = (f32[64,2]{0,1:T(2,128)S(1)}, f32[64,2]{0,1:T(2,128)}, u32[]{:S(2)}) copy-start(f32[64,2]{0,1:T(2,128)} %param.38) | copy-start | bytes 1540
  86.4 75.8 %copy-start.7 = (bf16[1024]{0:T(1024)(128)(2,1)S(1)}, bf16[1024]{0:T(1024)(128)(2,1)}, u32[]{:S(2)}) copy-start(bf16[1024]{0:T(1024)(128)(2,1)} %param.32) | copy-start | bytes 6148
  158.1 10.3 %all-to-all-start = ((bf16[16,16,1024]{2,1,0:T(8,128)(2,1)}), bf16[16,16,1024]{2,1,0:T(8,128)(2,1)S(1)}, u32[]{:S(2)}, u32[]{:S(2)}) async-start(bf16[16,16,1024]{2,1,0:T(8,128)(2,1)} %broadcast_select_fusion), calls=%async_computation.1 | async-start | bytes 1048576 | tf_op jit(solution)/shard_map/all_to_all | solution.py:125
  184.6 18.2 %copy-start.1 = (bf16[1024,512]{1,0:T(8,128)(2,1)S(1)}, bf16[1024,512]{1,0:T(8,128)(2,1)}, u32[]{:S(2)}) copy-start(bf16[1024,512]{1,0:T(8,128)(2,1)} %param.34) | copy-start | bytes 3145732
  199.3 17.6 %all-to-all-start.1 = ((f32[4,1,65536]{2,1,0:T(1,128)}), f32[4,1,65536]{2,1,0:T(1,128)S(1)}, u32[]{:S(2)}, u32[]{:S(2)}) async-start(f32[4,1,65536]{2,1,0:T(1,128)} %reshape.230), calls=%async_computation.2 | async-start | bytes 2097152 | tf_op jit(solution)/shard_map/all_to_all | solution.py:140
  202.8 47.6 %all-reduce.12.cloned.1.call-start = ((), (), s32[]{:S(2)}) async-start(), calls=%async_computation.6 | async-start | bytes 524288 | tf_op jit(solution)/shard_map/psum | solution.py:90
  206.0 102.0 %all-reduce.10.cloned.1.call-start = ((), (), s32[]{:S(2)}) async-start(), calls=%async_computation.5 | async-start | bytes 524288 | tf_op jit(solution)/shard_map/psum | solution.py:144
Sparse Core Ops, SparseCore 0:
  10.7 26.9 reduce-scatter.1
  99.2 55.6 all-reduce.7
  207.1 43.2 all-reduce.11
  252.6 55.4 all-reduce.9
where the time goes:
time: 317 us; the launch traced here: 316 us
  waiting for transfers between devices  129 us (41%)
  local copies, waits for them, and re-layouts  52.7 us (17%)
  other arithmetic  52.6 us (17%)
  matrix products  30.5 us (10%)
  blocking collectives  29.3 us (9%)
  between operations  14.8 us (5%)
  starting transfers between devices  7.33 us (2%)
    psum x1, waiting for transfers between devices, on_device(): attn_out = lax.psum(attn_part, 'tp')  55.8 us
    psum x1, waiting for transfers between devices, on_device(): result_sum = middle_float + lax.psum(expert_part + dense_part, 'tp')  55.6 us
    another operation x3, other arithmetic  40.5 us
    unnamed x30, local copies, waits for them, and re-layouts  18.6 us
    reshape x1, local copies, waits for them, and re-layouts, on_device(): head_keys = key_cache.reshape(seq_local, cache_len, heads_local, HD)  12.3 us
    psum x1, waiting for transfers between devices, on_device(): lax.psum((jnp.dot(scaled_mid, w_dense_gate, preferred_element_type=jnp.fl...  11.5 us
    unnamed x1, blocking collectives  11.5 us
    psum x1, blocking collectives, on_device(): lax.psum((jnp.dot(scaled_mid, w_dense_gate, preferred_element_type=jnp.fl...  10.6 us
  transfers between devices with their start and end apart: 6, of which 4 were waited for; matrix products, arithmetic and copies ran while one was open for 13% of the time, Pallas kernels for 0%

commit v1 on v0

--- a/solution.py
+++ b/solution.py
@@ -81,7 +81,9 @@
         w_output,
         preferred_element_type=jnp.float32,
     )
-    attn_out = lax.psum(attn_part, "tp")
+    attn_out = attn_part
+    for hop in (1, 2, 4):
+        attn_out = attn_out + lax.ppermute(attn_out, "tp", [(dev, dev ^ hop) for dev in range(8)])
     middle = (tokens_float + attn_out).astype(jnp.bfloat16)
     middle_float = middle.astype(jnp.float32)
     gain_float = gain_ffn.astype(jnp.float32)

time: 317 us -> 287 us (0.905)
  waiting for transfers between devices: 129 us -> 94.8 us
  starting transfers between devices: 7.33 us -> 11.4 us
    psum x1 -> x0, waiting for transfers between devices: 55.8 us -> none  [on_device(): attn_out = lax.psum(attn_part, 'tp')]
    ppermute x0 -> x3, waiting for transfers between devices: none -> 18.3 us  [on_device(): lax.ppermute(attn_out, 'tp', [(dev, dev ^ hop) for dev in range(8)])]
    ppermute x0 -> x3, starting transfers between devices: none -> 4.09 us  [on_device(): lax.ppermute(attn_out, 'tp', [(dev, dev ^ hop) for dev in range(8)])]
  transfers between devices with their start and end apart: 6 -> 8, of which waited for: 4 -> 7; matrix products, arithmetic and copies ran while one was open for 13% -> 14% of each run, Pallas kernels for 0% -> 0%
where the time goes in v1:
time: 287 us; the launch traced here: 286 us
  waiting for transfers between devices  94.8 us (33%)
  local copies, waits for them, and re-layouts  52.7 us (18%)
  other arithmetic  50.8 us (18%)
  blocking collectives  31.8 us (11%)
  matrix products  29.8 us (10%)
  between operations  14.8 us (5%)
  starting transfers between devices  11.4 us (4%)
    psum x1, waiting for transfers between devices, on_device(): result_sum = middle_float + lax.psum(expert_part + dense_part, 'tp')  55.7 us
    another operation x3, other arithmetic  40.5 us
    unnamed x30, local copies, waits for them, and re-layouts  18.6 us
    ppermute x3, waiting for transfers between devices, on_device(): lax.ppermute(attn_out, 'tp', [(dev, dev ^ hop) for dev in range(8)])  18.3 us
    psum x1, waiting for transfers between devices, on_device(): lax.psum((jnp.dot(scaled_mid, w_dense_gate, preferred_element_type=jnp.fl...  12.4 us
    reshape x1, local copies, waits for them, and re-layouts, on_device(): head_keys = key_cache.reshape(seq_local, cache_len, heads_local, HD)  12.3 us
    psum x1, blocking collectives, on_device(): lax.psum((jnp.dot(scaled_mid, w_dense_gate, preferred_element_type=jnp.fl...  12.1 us
    unnamed x1, blocking collectives  11.5 us
  transfers between devices with their start and end apart: 8, of which 7 were waited for; matrix products, arithmetic and copies ran while one was open for 14% of the time, Pallas kernels for 0%

profile of v1, /device:TPU:0, one launch (start us, length us, event | category | flops | bytes accessed | tf_op | source)
XLA Modules:
  0.0 286.0 jit_solution(1920667691176523613)
XLA Ops:
  7.2 0.8 convert_element_type.69
  8.0 2.5 fusion.3
  10.6 12.3 %copy.64 = bf16[16,1024,256]{1,2,0:T(8,128)(2,1)} copy(bf16[16,1024,256]{2,1,0:T(8,128)(2,1)} %param.27) | data formatting | bytes 16777216 | tf_op jit(solution)/shard_map/reshape | solution.py:65
  23.0 0.1 copy.50
  23.1 0.1 eq.19
  23.2 0.6 dynamic-slice
  24.4 0.1 fusion.41
  24.6 0.1 fusion.14
  24.7 11.5 %all-reduce.1 = f32[64]{0:T(128)S(1)} all-reduce(f32[64]{0:T(128)S(1)} %fusion.14), channel_id=3, replica_groups=mesh['ep'=4,'tp'=8] {'ep'}, use_global_device_ids=true, to_apply=%region_2.0.clone | all-reduce | flops 64 | bytes 512
  36.3 1.5 reduce-scatter.2.cloned.1.call-done
  37.7 0.9 multiply_convert_fusion.6
  38.6 0.6 fusion.57
  39.2 4.6 %fusion.58 = f32[16,2,1,1024]{3,2,1,0:T(1,128)S(1)} fusion(bf16[16,2,128,1]{2,3,1,0:T(2,128)(2,1)S(1)} %reshape.226, bf16[16,1024,2,128]{1,3,2,0:T(8,128)(2,1)} %bitcast.59), kind=kOutput, calls=%fused_computation.104 | convolution fusion | flops 8388608 | bytes 8527872 | tf_op jit(solution)/shard_map/bhd,blhd->bhl/dot_general | solution.py:66
  43.8 0.4 fusion.24
  44.2 0.1 reshape.188
  44.4 39.6 %reduce-window.6 = f32[16,2,8,128]{3,2,1,0:T(8,128)S(1)} reduce-window(f32[16,2,8,128]{3,2,1,0:T(8,128)S(1)} %reshape.188, f32[]{:T(128)} %constant.94.clone.1), window={size=1x1x1x128 pad=0_0x0_0x0_0x0_127}, to_apply=%region_3.4 | reduce-window | flops 4161536 | bytes 262148 | tf_op jit(solution)/shard_map/reduce-window
  84.0 0.2 copy.48
  84.3 0.1 broadcast_add_fusion
  84.5 0.8 fusion.42
  85.3 4.6 %fusion = f32[16,2,1,128]{3,2,1,0:T(1,128)S(1)} fusion(bf16[16,2,1024,1]{2,1,0,3:T(2,128)(2,1)S(1)} %fusion.42, bf16[16,1024,256]{2,1,0:T(8,128)(2,1)} %param.28), kind=kOutput, calls=%fused_computation.3 | convolution fusion | flops 8388608 | bytes 8470528 | tf_op jit(solution)/shard_map/bhl,blhd->bhd/dot_general | solution.py:77
  89.9 8.2 %all_gather.3 = bf16[64,256]{1,0:T(8,128)(2,1)S(1)} all-gather(bf16[16,256]{1,0:T(8,128)(2,1)S(1)} %bitcast.70), channel_id=1, replica_groups=mesh['ep'=4,'tp'=8] {'ep'}, dimensions={0}, use_global_device_ids=true | all-gather | bytes 40960 | tf_op jit(solution)/shard_map/all_gather | solution.py:80
  98.1 0.2 fusion.59
  98.4 0.2 select_reduce_fusion
  98.6 0.1 reduce_sum.59
  98.7 0.1 copy.53
  98.8 0.1 mul.169
  99.0 1.0 collective-permute-done
  100.0 1.6 collective-permute-start.1
  101.5 1.0 scatter_custom_fusion
  102.5 0.1 broadcast_in_dim.46
  102.6 5.8 %collective-permute-done.1 = f32[64,1024]{1,0:T(8,128)S(1)} collective-permute-done((f32[64,1024]{1,0:T(8,128)S(1)}, f32[64,1024]{1,0:T(8,128)S(1)}, u32[]{:S(2)}, u32[]{:S(2)}) %collective-permute-start.1) | collective-permute-done | bytes 262176 | tf_op jit(solution)/shard_map/ppermute | solution.py:86
  108.4 2.5 collective-permute-start.2
  110.9 11.6 %collective-permute-done.2 = f32[64,1024]{1,0:T(8,128)S(1)} collective-permute-done((f32[64,1024]{1,0:T(8,128)S(1)}, f32[64,1024]{1,0:T(8,128)S(1)}, u32[]{:S(2)}, u32[]{:S(2)}) %collective-permute-start.2) | collective-permute-done | bytes 262176 | tf_op jit(solution)/shard_map/ppermute | solution.py:86
  122.5 0.1 fusion.17
  122.6 1.2 gather_fusion
  123.8 0.9 broadcast_select_fusion
  124.7 3.6 %all-to-all-start = ((bf16[16,16,1024]{2,1,0:T(8,128)(2,1)}), bf16[16,16,1024]{2,1,0:T(8,128)(2,1)S(1)}, u32[]{:S(2)}, u32[]{:S(2)}) async-start(bf16[16,16,1024]{2,1,0:T(8,128)(2,1)} %broadcast_select_fusion), calls=%async_computation.1 | async-start | bytes 1048576 | tf_op jit(solution)/shard_map/all_to_all | solution.py:127
  128.4 0.1 reduce_sum.58
  128.6 0.1 copy.52
  128.7 0.1 copy.57
  128.9 6.8 %all-to-all-done = bf16[16,16,1024]{2,1,0:T(8,128)(2,1)S(1)} async-done(((bf16[16,16,1024]{2,1,0:T(8,128)(2,1)}), bf16[16,16,1024]{2,1,0:T(8,128)(2,1)S(1)}, u32[]{:S(2)}, u32[]{:S(2)}) %all-to-all-start) | async-done | bytes 524320 | tf_op jit(solution)/shard_map/all_to_all | solution.py:127
  135.7 1.5 copy.82
  137.2 1.9 reshape.192
  139.1 0.2 multiply_reduce_fusion
  139.3 4.5 %convolution_multiply_fusion.2 = f32[4,16,256]{2,1,0:T(8,128)S(1)} fusion(bf16[4,4096,256]{2,1,0:T(8,128)(2,1)} %param.39, f32[4,16,4096]{2,1,0:T(8,128)S(1)} %reshape.192, f32[4096]{0:T(1024)S(1)} %convert_element_type.81, f32[4,16]{1,0:T(4,128)S(1)} %add_rsqrt_fusion), kind=kOutput, calls=%fused_computation.16 | convolution fusion | flops 134758400 | bytes 9519360 | tf_op jit(solution)/shard_map/end,edf->enf/dot_general | solution.py:133
  143.9 8.1 %fusion.12 = f32[4,16,4096]{2,1,0:T(8,128)S(1)} fusion(bf16[4,256,4096]{2,1,0:T(8,128)(2,1)} %param.41, bf16[4,4096,256]{2,1,0:T(8,128)(2,1)} %param.40, f32[4,16,4096]{2,1,0:T(8,128)S(1)} %reshape.192, f32[4096]{0:T(1024)S(1)} %convert_element_type.81, f32[4,16,256]{2,1,0:T(8,128)S(1)} %convolution_multiply_fusion.2, f32[4,16]{1,0:T(4,128)S(1)} %add_rsqrt_fusion), kind=kOutput, calls=%fused_computation.22 | convolution fusion | flops 269074432 | bytes 18956544 | tf_op jit(solution)/shard_map/enf,efd->end/dot_general | solution.py:141
  152.0 5.9 %copy.55 = f32[4,16,4096]{1,0,2:T(4,128)} copy(f32[4,16,4096]{2,1,0:T(8,128)S(1)} %fusion.12) | data formatting | bytes 2097152 | tf_op jit(solution)/shard_map/enf,efd->end/dot_general | solution.py:141
  157.8 8.8 %reshape.230 = f32[4,1,65536]{2,1,0:T(1,128)} reshape(f32[4096,4,16]{2,1,0:T(4,128)} %bitcast.60) | data formatting | bytes 2097152
  166.6 3.5 %all-to-all-start.1 = ((f32[4,1,65536]{2,1,0:T(1,128)}), f32[4,1,65536]{2,1,0:T(1,128)S(1)}, u32[]{:S(2)}, u32[]{:S(2)}) async-start(f32[4,1,65536]{2,1,0:T(1,128)} %reshape.230), calls=%async_computation.2 | async-start | bytes 2097152 | tf_op jit(solution)/shard_map/all_to_all | solution.py:142
  170.2 0.9 fusion.30
  171.2 2.2 fusion.32
  173.4 0.1 convolution_bitcast_fusion
  173.5 12.1 %all-reduce.2 = (f32[64]{0:T(128)S(1)}, f32[64]{0:T(128)S(1)}) all-reduce(f32[64]{0:T(128)S(1)} %convolution_bitcast_fusion, f32[64]{0:T(128)S(1)} %get-tuple-element.7), channel_id=1, replica_groups=mesh['ep'=4,'tp'=8] {'ep'}, use_global_device_ids=true, to_apply=%region_15.16 | all-reduce | flops 128 | bytes 1024 | tf_op jit(solution)/shard_map/psum | solution.py:92
  185.7 0.6 broadcast.214
  186.3 3.7 %reduce.5 = f32[4,65536]{1,0:T(4,128)S(1)} reduce(f32[4,1,65536]{2,1,0:T(1,128)S(1)} %all-to-all-done.1, f32[]{:T(128)} %broadcast.214), dimensions={1}, to_apply=%all_to_all.9.reduce_sub_computation | reduce | bytes 2097156 | tf_op jit(solution)/shard_map/all_to_all | solution.py:142
  190.0 9.1 %reshape.231 = f32[4096,4,16]{2,1,0:T(4,128)} reshape(f32[4,65536]{1,0:T(4,128)S(1)} %reduce.5) | data formatting | bytes 2097152
  199.1 6.7 %copy.56 = f32[4,16,4,1024]{3,1,0,2:T(8,128)S(1)} copy(f32[4,16,4,1024]{1,0,3,2:T(4,128)} %bitcast.61) | data formatting | bytes 2097152 | tf_op jit(solution)/shard_map/all_to_all | solution.py:142
  205.8 0.8 gather_fusion.1
  206.6 0.3 gather.15
  206.9 0.8 multiply_reduce_fusion.1
  207.7 12.4 %all-reduce.9.cloned.1.call-done = (f32[64,512]{1,0:T(8,128)}, f32[64,512]{1,0:T(8,128)}) async-done(((f32[64,512]{1,0:T(8,128)}, f32[64,512]{1,0:T(8,128)}), (f32[64,512]{1,0:T(8,128)}, f32[64,512]{1,0:T(8,128)})) %all-reduce.9.cloned.1.call-update) | async-done | bytes 262160 | tf_op jit(solution)/shard_map/psum | solution.py:92
  220.1 2.0 fusion.9
  222.1 55.7 %all-reduce.7.cloned.1.call-done = f32[64,1024]{1,0:T(8,128)} async-done(((f32[64,1024]{1,0:T(8,128)}), f32[64,1024]{1,0:T(8,128)}) %all-reduce.7.cloned.1.call-update) | async-done | bytes 262160 | tf_op jit(solution)/shard_map/psum | solution.py:146
  277.9 1.6 fusion.18
  (60 shorter events, 1.0 us)
Async XLA Ops:
  7.2 212.9 %copy-start = (bf16[512,1024]{1,0:T(8,128)(2,1)S(1)}, bf16[512,1024]{1,0:T(8,128)(2,1)}, u32[]{:S(2)}) copy-start(bf16[512,1024]{1,0:T(8,128)(2,1)} %param.35) | copy-start | bytes 3145732
  7.2 30.6 %reduce-scatter.2.cloned.1.call-start = ((), (), s32[]{:S(2)}) async-start(), calls=%async_computation.3 | async-start | bytes 245760 | tf_op jit(solution)/shard_map/reduce_scatter | solution.py:52
  10.5 12.4 %copy-start.10 = (s32[64]{0:T(128)S(1)}, s32[64]{0:T(128)}, u32[]{:S(2)}) copy-start(s32[64]{0:T(128)} %param.36) | copy-start | bytes 772
  10.5 12.4 %copy-start.8 = (s32[64,2]{0,1:T(2,128)S(1)}, s32[64,2]{0,1:T(2,128)}, u32[]{:S(2)}) copy-start(s32[64,2]{0,1:T(2,128)} %param.37) | copy-start | bytes 1540
  10.6 12.6 %copy-start.11 = (u32[32]{0:T(128)S(1)}, u32[32]{0:T(128)}, u32[]{:S(2)}) copy-start(u32[32]{0:T(128)} %constant.122) | copy-start | bytes 388
  10.6 14.0 %copy-start.3 = (bf16[64,1024]{1,0:T(8,128)(2,1)S(1)}, bf16[64,1024]{1,0:T(8,128)(2,1)}, u32[]{:S(2)}) copy-start(bf16[64,1024]{1,0:T(8,128)(2,1)} %param.21) | copy-start | bytes 393220
  22.9 20.9 %copy-start.5 = (s32[16]{0:T(128)S(1)}, s32[16]{0:T(128)}, u32[]{:S(2)}) copy-start(s32[16]{0:T(128)} %param.29) | copy-start | bytes 196
  22.9 20.9 %copy-start.6 = (f32[2]{0:T(128)S(1)}, f32[2]{0:T(128)}, u32[]{:S(2)}) copy-start(f32[2]{0:T(128)} %param.30) | copy-start | bytes 28
  43.8 54.3 %copy-start.2 = (bf16[256,1024]{1,0:T(8,128)(2,1)S(1)}, bf16[256,1024]{1,0:T(8,128)(2,1)}, u32[]{:S(2)}) copy-start(bf16[256,1024]{1,0:T(8,128)(2,1)} %param.26) | copy-start | bytes 1572868
  85.3 43.2 %copy-start.4 = (bf16[4096]{0:T(1024)(128)(2,1)S(1)}, bf16[4096]{0:T(1024)(128)(2,1)}, u32[]{:S(2)}) copy-start(bf16[4096]{0:T(1024)(128)(2,1)} %param.31) | copy-start | bytes 24580
  85.3 43.4 %copy-start.9 = (f32[64,2]{0,1:T(2,128)S(1)}, f32[64,2]{0,1:T(2,128)}, u32[]{:S(2)}) copy-start(f32[64,2]{0,1:T(2,128)} %param.38) | copy-start | bytes 1540
  85.3 43.5 %copy-start.7 = (bf16[1024]{0:T(1024)(128)(2,1)S(1)}, bf16[1024]{0:T(1024)(128)(2,1)}, u32[]{:S(2)}) copy-start(bf16[1024]{0:T(1024)(128)(2,1)} %param.32) | copy-start | bytes 6148
  98.3 1.6 collective-permute-start
  100.0 8.4 %collective-permute-start.1 = (f32[64,1024]{1,0:T(8,128)S(1)}, f32[64,1024]{1,0:T(8,128)S(1)}, u32[]{:S(2)}, u32[]{:S(2)}) collective-permute-start(f32[64,1024]{1,0:T(8,128)S(1)} %add.174), channel_id=1, source_target_pairs={{0,2},{1,3},{2,0},{3,1},{4,6},{5,7},{6,4},{7,5},{8,10},{9,11},{10,... | collective-permute-start | bytes 786440 | tf_op jit(solution)/shard_map/ppermute | solution.py:86
  108.4 14.1 %collective-permute-start.2 = (f32[64,1024]{1,0:T(8,128)S(1)}, f32[64,1024]{1,0:T(8,128)S(1)}, u32[]{:S(2)}, u32[]{:S(2)}) collective-permute-start(f32[64,1024]{1,0:T(8,128)S(1)} %add.175), channel_id=1, source_target_pairs={{0,4},{1,5},{2,6},{3,7},{4,0},{5,1},{6,2},{7,3},{8,12},{9,13},{10,... | collective-permute-start | bytes 786440 | tf_op jit(solution)/shard_map/ppermute | solution.py:86
  124.7 11.0 %all-to-all-start = ((bf16[16,16,1024]{2,1,0:T(8,128)(2,1)}), bf16[16,16,1024]{2,1,0:T(8,128)(2,1)S(1)}, u32[]{:S(2)}, u32[]{:S(2)}) async-start(bf16[16,16,1024]{2,1,0:T(8,128)(2,1)} %broadcast_select_fusion), calls=%async_computation.1 | async-start | bytes 1048576 | tf_op jit(solution)/shard_map/all_to_all | solution.py:127
  152.0 18.2 %copy-start.1 = (bf16[1024,512]{1,0:T(8,128)(2,1)S(1)}, bf16[1024,512]{1,0:T(8,128)(2,1)}, u32[]{:S(2)}) copy-start(bf16[1024,512]{1,0:T(8,128)(2,1)} %param.34) | copy-start | bytes 3145732
  166.6 19.1 %all-to-all-start.1 = ((f32[4,1,65536]{2,1,0:T(1,128)}), f32[4,1,65536]{2,1,0:T(1,128)S(1)}, u32[]{:S(2)}, u32[]{:S(2)}) async-start(f32[4,1,65536]{2,1,0:T(1,128)} %reshape.230), calls=%async_computation.2 | async-start | bytes 2097152 | tf_op jit(solution)/shard_map/all_to_all | solution.py:142
  170.1 49.9 %all-reduce.9.cloned.1.call-start = ((), (), s32[]{:S(2)}) async-start(), calls=%async_computation.5 | async-start | bytes 524288 | tf_op jit(solution)/shard_map/psum | solution.py:92
  173.3 104.5 %all-reduce.7.cloned.1.call-start = ((), (), s32[]{:S(2)}) async-start(), calls=%async_computation.4 | async-start | bytes 524288 | tf_op jit(solution)/shard_map/psum | solution.py:146
Sparse Core Ops, SparseCore 0:
  10.7 26.9 reduce-scatter.1
  174.4 45.5 all-reduce.8
  222.4 55.4 all-reduce.6
